TPU v7x, 32 devices: a whole 2x2x4 slice. The times are simulated.
32 devices in a mesh: sp: 8 (over z, y), tp: 4 (over x, core).
Axes of the slice: x: 2, y: 2, z: 4, core: 2. Of those that a mesh axis runs over, the one named last changes fastest.
Arguments:
- resid: bfloat16 [2048, 2048], P(('sp', 'tp')), may hold values from -0.21875 to 0.21875
- query_a: bfloat16 [2048, 1024], P('sp', 'tp'), may hold values from -6 to 6
- key_a: bfloat16 [2048, 256], P('sp', 'tp'), may hold values from -6 to 6
- value_a: bfloat16 [2048, 256], P('sp', 'tp'), may hold values from -6 to 6
- query_b: bfloat16 [2048, 1024], P('sp', 'tp'), may hold values from -6 to 6
- key_b: bfloat16 [2048, 512], P('sp', 'tp'), may hold values from -6 to 6
- value_b: bfloat16 [2048, 512], P('sp', 'tp'), may hold values from -6 to 6
- gain_qa: float32 [64], replicated, may hold values from 0.1 to 8
- gain_ka: float32 [64], replicated, may hold values from 0.1 to 8
- gain_qb: float32 [128], replicated, may hold values from 0.1 to 8
- gain_kb: float32 [128], replicated, may hold values from 0.1 to 8
- w_out_a: bfloat16 [1024, 2048], P('tp'), may hold values from -0.125 to 0.125
- w_out_b: bfloat16 [1024, 2048], P('tp'), may hold values from -0.125 to 0.125
- norm_gain: float32 [2048], replicated, may hold values from 0.1 to 1.9
- w_up: bfloat16 [2048, 8192], P('sp', 'tp'), may hold values from -0.125 to 0.125
- w_down: bfloat16 [8192, 2048], P('tp', 'sp'), may hold values from -0.0625 to 0.0625
Outputs:
- result: bfloat16 [2048, 2048], P(('sp', 'tp'))
All inputs are finite; a program needn't handle non-finite values.
Results may differ from a plain program's by a relative error of at most 0.02.
The roundings to bfloat16 on the way count: a program that leaves them out, or rounds other values in their place, can miss the bound.
Values may be sent and summed in bfloat16 or wider, within the bound.
A program may use at most 128 MiB of HBM per device.

v0:
```python
import math
import jax
import jax.numpy as jnp
from jax import lax
from jax.sharding import PartitionSpec as P

GRID_W = 64
EPS = 1e-06


def norm_rope(values, gain, places):
    width = gain.shape[0]
    count = values.shape[0]
    flat = values.astype(jnp.float32).reshape(count, -1, width)
    flat = flat * lax.rsqrt(jnp.mean(flat * flat, axis=-1, keepdims=True) + EPS) * gain
    grid_rows = (places // GRID_W).astype(jnp.float32)
    grid_cols = (places % GRID_W).astype(jnp.float32)
    quarter = width // 4
    freqs = 10000.0 ** (-(2.0 * jnp.arange(quarter, dtype=jnp.float32)) / (width // 2))
    ang_r = grid_rows[:, None] * freqs
    ang_c = grid_cols[:, None] * freqs
    angles = jnp.concatenate([ang_r, ang_r, ang_c, ang_c], axis=-1)
    one, two, three, four = jnp.split(flat, 4, axis=-1)
    turned = jnp.concatenate([-two, one, -four, three], axis=-1)
    return (flat * jnp.cos(angles)[:, None, :] + turned * jnp.sin(angles)[:, None, :]).astype(
        jnp.bfloat16
    )


def fold_block(state, queries, key_block, value_block, scale):
    running, total, accum = state
    scores = (
        jnp.einsum("rkgd,pkd->kgrp", queries, key_block, preferred_element_type=jnp.float32) * scale
    )
    newest = jnp.maximum(running, jnp.max(scores, axis=-1))
    factor = jnp.exp(running - newest)
    expo = jnp.exp(scores - newest[..., None])
    total = total * factor + jnp.sum(expo, axis=-1)
    accum = accum * factor[..., None] + jnp.einsum(
        "kgrp,pkd->kgrd", expo.astype(jnp.bfloat16), value_block, preferred_element_type=jnp.float32
    )
    return (newest, total, accum)


def sweep_keys(state, queries, key_piece, value_piece, scale):
    length = key_piece.shape[0]
    block = math.gcd(length, 2048)
    blocks = length // block
    if blocks == 1:
        return fold_block(state, queries, key_piece, value_piece, scale)
    key_blocks = key_piece.reshape((blocks, block) + key_piece.shape[1:])
    value_blocks = value_piece.reshape((blocks, block) + value_piece.shape[1:])

    def advance(carry, pair):
        return (fold_block(carry, queries, pair[0], pair[1], scale), None)

    state, unused = lax.scan(advance, state, (key_blocks, value_blocks))
    return state


def start_state(queries):
    shape = (queries.shape[1], queries.shape[2], queries.shape[0])
    return (
        jnp.full(shape, -1e30, jnp.float32),
        jnp.zeros(shape, jnp.float32),
        jnp.zeros(shape + (queries.shape[3],), jnp.float32),
    )


def finish(state):
    running, total, accum = state
    outputs = accum / total[..., None]
    count = outputs.shape[2]
    return jnp.transpose(outputs, (2, 0, 1, 3)).reshape(count, -1).astype(jnp.bfloat16)


def local(
    resid,
    query_a,
    key_a,
    value_a,
    query_b,
    key_b,
    value_b,
    gain_qa,
    gain_ka,
    gain_qb,
    gain_kb,
    w_out_a,
    w_out_b,
    norm_gain,
    w_up,
    w_down,
):
    count = query_a.shape[0]
    width_a = gain_qa.shape[0]
    width_b = gain_qb.shape[0]
    places = lax.axis_index("sp") * count + jnp.arange(count, dtype=jnp.int32)
    keys_a = norm_rope(key_a, gain_ka, places)
    keys_b = norm_rope(key_b, gain_kb, places)
    heads_kv_a = keys_a.shape[1]
    heads_kv_b = keys_b.shape[1]
    queries_a = norm_rope(query_a, gain_qa, places)
    queries_b = norm_rope(query_b, gain_qb, places)
    queries_a = queries_a.reshape(count, heads_kv_a, queries_a.shape[1] // heads_kv_a, width_a)
    queries_b = queries_b.reshape(count, heads_kv_b, queries_b.shape[1] // heads_kv_b, width_b)
    values_a = value_a.reshape(count, heads_kv_a, width_a)
    values_b = value_b.reshape(count, heads_kv_b, width_b)
    state_a = sweep_keys(
        start_state(queries_a),
        queries_a,
        lax.all_gather(keys_a, "sp", axis=0, tiled=True),
        lax.all_gather(values_a, "sp", axis=0, tiled=True),
        width_a ** (-0.5),
    )
    state_b = sweep_keys(
        start_state(queries_b),
        queries_b,
        lax.all_gather(keys_b, "sp", axis=0, tiled=True),
        lax.all_gather(values_b, "sp", axis=0, tiled=True),
        width_b ** (-0.5),
    )
    attn_a = finish(state_a)
    attn_b = finish(state_b)
    rows_a, rows_b = (
        lax.all_to_all(attn_a, "tp", split_axis=0, concat_axis=1, tiled=True),
        lax.all_to_all(attn_b, "tp", split_axis=0, concat_axis=1, tiled=True),
    )
    whole_a, whole_b = (
        lax.all_gather(w_out_a, "tp", axis=0, tiled=True),
        lax.all_gather(w_out_b, "tp", axis=0, tiled=True),
    )
    proj = jnp.dot(rows_a, whole_a, preferred_element_type=jnp.float32) + jnp.dot(
        rows_b, whole_b, preferred_element_type=jnp.float32
    )
    mid = (resid.astype(jnp.float32) + proj).astype(jnp.bfloat16)
    midf = mid.astype(jnp.float32)
    normed = (
        midf * lax.rsqrt(jnp.mean(midf * midf, axis=-1, keepdims=True) + EPS) * norm_gain
    ).astype(jnp.bfloat16)
    up_whole, down_whole = (
        lax.all_gather(w_up, "sp", axis=0, tiled=True),
        lax.all_gather(w_down, "sp", axis=1, tiled=True),
    )
    hidden = jnp.square(
        jax.nn.relu(
            jnp.dot(
                lax.all_gather(normed, "tp", axis=0, tiled=True),
                up_whole,
                preferred_element_type=jnp.float32,
            )
        )
    ).astype(jnp.bfloat16)
    mixed = lax.psum_scatter(
        jnp.dot(hidden, down_whole, preferred_element_type=jnp.float32).astype(jnp.bfloat16),
        "tp",
        scatter_dimension=0,
        tiled=True,
    ).astype(jnp.float32)
    return (midf + mixed).astype(jnp.bfloat16)


def solution(mesh):
    return jax.shard_map(
        local,
        mesh=mesh,
        in_specs=(
            P(("sp", "tp"), None),
            P("sp", "tp"),
            P("sp", "tp"),
            P("sp", "tp"),
            P("sp", "tp"),
            P("sp", "tp"),
            P("sp", "tp"),
            P(),
            P(),
            P(),
            P(),
            P("tp", None),
            P("tp", None),
            P(),
            P("sp", "tp"),
            P("tp", "sp"),
        ),
        out_specs=P(("sp", "tp"), None),
        check_vma=False,
    )
```

profile of v0, /device:TPU:0, one launch (start us, length us, event | category | flops | bytes accessed | tf_op | source)
XLA Modules:
  0.0 480.9 jit_solution(12184441608509386701)
XLA Ops:
  6.5 0.7 all-gather.10.cloned.1.call-update
  7.3 0.7 all-gather.12.cloned.1.call-update
  8.1 1.0 fusion.53
  9.0 0.9 fusion.55
  10.0 0.2 fusion.63
  10.2 1.1 reshape.505
  11.3 0.3 multiply_reduce_fusion.1
  11.7 0.3 multiply_multiply_fusion
  12.0 0.9 slice_negate_fusion.1
  12.9 0.1 broadcast_multiply_fusion.1
  13.0 0.6 fusion.58
  13.7 33.2 %all-gather.2 = bf16[2048,128]{1,0:T(8,128)(2,1)S(1)} all-gather(bf16[256,128]{1,0:T(8,128)(2,1)S(1)} %get-tuple-element.5), channel_id=4, replica_groups=mesh['sp'=8,'tp'=4] {'sp'}, dimensions={0}, use_global_device_ids=true | all-gather | bytes 589824 | tf_op jit(solution)/shard_map/all_gather | solution.py:119
  46.9 0.9 maximum_multiply_fusion.1
  47.8 0.1 mul.427
  47.9 0.3 mul.420
  48.2 0.8 bitcast_reduce_fusion.1
  49.0 0.7 fusion.7
  49.8 31.4 %all-gather.3 = bf16[2048,128]{1,0:T(8,128)(2,1)S(1)} all-gather(bf16[256,128]{1,0:T(8,128)(2,1)S(1)} %copy-done.5), channel_id=5, replica_groups=mesh['sp'=8,'tp'=4] {'sp'}, dimensions={0}, use_global_device_ids=true | all-gather | bytes 589824 | tf_op jit(solution)/shard_map/all_gather | solution.py:120
  81.2 0.9 fusion.31
  82.1 0.1 copy.48
  82.2 0.7 convert_element_type.140
  83.0 3.3 all-to-all-start.1
  86.3 0.1 copy.40
  86.4 0.1 mul.388
  86.7 0.1 fusion.66
  86.8 0.1 fusion.69
  87.0 0.1 multiply_multiply_fusion.1
  87.1 0.1 fusion.49
  87.2 30.7 %all-gather = bf16[2048,64]{0,1:T(8,128)(2,1)S(1)} all-gather(bf16[256,64]{0,1:T(8,128)(2,1)S(1)} %get-tuple-element.26), channel_id=2, replica_groups=mesh['sp'=8,'tp'=4] {'sp'}, dimensions={0}, use_global_device_ids=true | all-gather | bytes 294912 | tf_op jit(solution)/shard_map/all_gather | solution.py:112
  118.0 30.9 %all-gather.1 = bf16[2048,64]{0,1:T(8,128)(2,1)S(1)} all-gather(bf16[256,64]{0,1:T(8,128)(2,1)S(1)} %copy-done.6), channel_id=3, replica_groups=mesh['sp'=8,'tp'=4] {'sp'}, dimensions={0}, use_global_device_ids=true | all-gather | bytes 294912 | tf_op jit(solution)/shard_map/all_gather | solution.py:113
  148.9 1.3 bitcast_reduce_fusion
  150.2 1.4 fusion.1
  151.6 1.5 fusion.40
  153.1 0.2 reshape.521
  153.3 0.8 copy.52
  154.1 3.3 all-to-all-start
  157.5 4.5 all-to-all-done
  162.1 3.0 fusion.86
  165.2 3.2 multiply_reduce_fusion
  168.4 0.8 multiply_convert_fusion
  169.3 0.5 all-gather.16.cloned.1.call-update
  169.9 0.5 all-gather.18.cloned.1.call-update
  170.5 15.7 %all-gather.14.cloned.1.call-done = bf16[256,2048]{1,0:T(8,128)(2,1)} async-done(((bf16[64,2048]{1,0:T(8,128)(2,1)}), bf16[256,2048]{1,0:T(8,128)(2,1)}) %all-gather.14.cloned.1.call-update) | async-done | bytes 1048592 | tf_op jit(solution)/shard_map/all_gather | solution.py:148
  186.2 126.5 %all-gather.16.cloned.1.call-done = bf16[2048,2048]{1,0:T(8,128)(2,1)} async-done(((bf16[256,2048]{1,0:T(8,128)(2,1)}), bf16[2048,2048]{1,0:T(8,128)(2,1)}) %all-gather.16.cloned.1.call-update) | async-done | bytes 8388624 | tf_op jit(solution)/shard_map/all_gather | solution.py:142
  312.7 125.0 %all-gather.18.cloned.1.call-done = bf16[2048,2048]{1,0:T(8,128)(2,1)} async-done(((bf16[2048,256]{1,0:T(8,128)(2,1)}), bf16[2048,2048]{1,0:T(8,128)(2,1)}) %all-gather.18.cloned.1.call-update) | async-done | bytes 8388624 | tf_op jit(solution)/shard_map/all_gather | solution.py:143
  437.7 11.5 %convolution_convert_fusion = bf16[256,2048]{1,0:T(8,128)(2,1)} fusion(bf16[2048,2048]{1,0:T(8,128)(2,1)} %all-gather.18.cloned.1.call-done, bf16[256,2048]{1,0:T(8,128)(2,1)} %all-gather.14.cloned.1.call-done, bf16[2048,2048]{1,0:T(8,128)(2,1)} %all-gather.16.cloned.1.call-done), kind=kOutput, calls=%fused_computation.15 | convolution fusion | flops 4297064448 | bytes 18874368 | tf_op jit(solution)/shard_map/dot_general | solution.py:155
  449.3 23.1 %reduce-scatter.2.cloned.1.call-done = bf16[64,2048]{1,0:T(8,128)(2,1)} async-done(((bf16[256,2048]{1,0:T(8,128)(2,1)}), bf16[64,2048]{1,0:T(8,128)(2,1)}) %reduce-scatter.2.cloned.1.call-update) | async-done | bytes 262160 | tf_op jit(solution)/shard_map/reduce_scatter | solution.py:154
  472.4 1.7 add_convert_fusion
  (57 shorter events, 0.7 us)
Async XLA Ops:
  6.5 6.5 %copy-start = (bf16[256,128]{1,0:T(8,128)(2,1)S(1)}, bf16[256,128]{1,0:T(8,128)(2,1)}, u32[]{:S(2)}) copy-start(bf16[256,128]{1,0:T(8,128)(2,1)} %param.21) | copy-start | bytes 196612
  6.5 6.5 %copy-start.8 = (f32[128]{0:T(128)S(1)}, f32[128]{0:T(128)}, u32[]{:S(2)}) copy-start(f32[128]{0:T(128)} %param.26) | copy-start | bytes 1540
  6.5 5.1 %copy-start.11 = (f32[128]{0:T(128)S(1)}, f32[128]{0:T(128)}, u32[]{:S(2)}) copy-start(f32[128]{0:T(128)} %param.25) | copy-start | bytes 1540
  6.5 155.6 %all-gather.10.cloned.1.call-start = ((), (), s32[]{:S(2)}) async-start(), calls=%async_computation.3 | async-start | bytes 5242880 | tf_op jit(solution)/shard_map/all_gather | solution.py:130
  7.3 157.9 %all-gather.12.cloned.1.call-start = ((), (), s32[]{:S(2)}) async-start(), calls=%async_computation.4 | async-start | bytes 5242880 | tf_op jit(solution)/shard_map/all_gather | solution.py:131
  10.1 38.1 %copy-start.1 = (bf16[256,256]{1,0:T(8,128)(2,1)S(1)}, bf16[256,256]{1,0:T(8,128)(2,1)}, u32[]{:S(2)}) copy-start(bf16[256,256]{1,0:T(8,128)(2,1)} %param.20) | copy-start | bytes 393220
  48.2 1.5 copy-start.5
  49.7 36.6 %copy-start.4 = (bf16[256,256]{1,0:T(8,128)(2,1)S(1)}, bf16[256,256]{1,0:T(8,128)(2,1)}, u32[]{:S(2)}) copy-start(bf16[256,256]{1,0:T(8,128)(2,1)} %param.17) | copy-start | bytes 393220
  49.7 36.7 %copy-start.10 = (f32[64]{0:T(128)S(1)}, f32[64]{0:T(128)}, u32[]{:S(2)}) copy-start(f32[64]{0:T(128)} %param.23) | copy-start | bytes 772
  49.7 36.8 %copy-start.2 = (bf16[256,64]{0,1:T(8,128)(2,1)S(1)}, bf16[256,64]{0,1:T(8,128)(2,1)}, u32[]{:S(2)}) copy-start(bf16[256,64]{0,1:T(8,128)(2,1)} %param.18) | copy-start | bytes 98308
  49.7 37.0 %copy-start.9 = (f32[64]{0:T(128)S(1)}, f32[64]{0:T(128)}, u32[]{:S(2)}) copy-start(f32[64]{0:T(128)} %param.24) | copy-start | bytes 772
  81.2 36.8 %copy-start.6 = (bf16[256,64]{0,1:T(8,128)(2,1)S(1)}, bf16[256,64]{0,1:T(8,128)(2,1)}, u32[]{:S(2)}) copy-start(bf16[256,64]{0,1:T(8,128)(2,1)} %param.19) | copy-start | bytes 98308
  83.0 71.1 %all-to-all-start.1 = ((bf16[4,64,256]{2,1,0:T(8,128)(2,1)}), bf16[4,64,256]{2,1,0:T(8,128)(2,1)S(1)}, u32[]{:S(2)}, u32[]{:S(2)}) async-start(bf16[4,64,256]{2,1,0:T(8,128)(2,1)} %convert_element_type.140), calls=%async_computation.1 | async-start | bytes 262144 | tf_op jit(solution)/shard_map/all_to_all | solution.py:127
  153.1 12.1 %copy-start.3 = (bf16[64,2048]{1,0:T(8,128)(2,1)S(1)}, bf16[64,2048]{1,0:T(8,128)(2,1)}, u32[]{:S(2)}) copy-start(bf16[64,2048]{1,0:T(8,128)(2,1)} %param.16) | copy-start | bytes 786436
  154.1 7.9 %all-to-all-start = ((bf16[4,64,256]{2,1,0:T(8,128)(2,1)}), bf16[4,64,256]{2,1,0:T(8,128)(2,1)S(1)}, u32[]{:S(2)}, u32[]{:S(2)}) async-start(bf16[4,64,256]{2,1,0:T(8,128)(2,1)} %copy.52), calls=%async_computation | async-start | bytes 262144 | tf_op jit(solution)/shard_map/all_to_all | solution.py:126
  157.5 28.7 %all-gather.14.cloned.1.call-start = ((), (), s32[]{:S(2)}) async-start(), calls=%async_computation.5 | async-start | bytes 1310720 | tf_op jit(solution)/shard_map/all_gather | solution.py:148
  162.1 6.3 %copy-start.7 = (f32[2048]{0:T(1024)S(1)}, f32[2048]{0:T(1024)}, u32[]{:S(2)}) copy-start(f32[2048]{0:T(1024)} %param.29) | copy-start | bytes 24580
  169.3 143.4 %all-gather.16.cloned.1.call-start = ((), (), s32[]{:S(2)}) async-start(), calls=%async_computation.6 | async-start | bytes 9437184 | tf_op jit(solution)/shard_map/all_gather | solution.py:142
  169.8 267.9 %all-gather.18.cloned.1.call-start = ((), (), s32[]{:S(2)}) async-start(), calls=%async_computation.7 | async-start | bytes 9437184 | tf_op jit(solution)/shard_map/all_gather | solution.py:143
  170.4 301.9 %reduce-scatter.2.cloned.1.call-start = ((), (), s32[]{:S(2)}) async-start(), calls=%async_computation.8 | async-start | bytes 1310720 | tf_op jit(solution)/shard_map/reduce_scatter | solution.py:154
Sparse Core Ops, SparseCore 0:
  8.9 37.1 all-gather.9
  47.7 34.4 all-gather.11
  169.4 16.7 all-gather.13
  188.1 124.4 all-gather.15
  314.6 123.1 all-gather.17
  449.4 22.9 reduce-scatter.1
where the time goes:
time: 481 us
  waiting for transfers between devices  297 us (62%)
  blocking collectives  126 us (26%)
  matrix products  22.3 us (5%)
  between operations  13.9 us (3%)
  other arithmetic  10.6 us (2%)
  starting transfers between devices  6.86 us (1%)
    all_gather x1, waiting for transfers between devices, local(): lax.all_gather(w_up, 'sp', axis=0, tiled=True)  126 us
    all_gather x1, waiting for transfers between devices, local(): lax.all_gather(w_down, 'sp', axis=1, tiled=True)  125 us
    all_gather x1, blocking collectives, local(): lax.all_gather(keys_b, 'sp', axis=0, tiled=True)  33.2 us
    all_gather x1, blocking collectives, local(): lax.all_gather(values_b, 'sp', axis=0, tiled=True)  31.4 us
    all_gather x1, blocking collectives, local(): lax.all_gather(values_a, 'sp', axis=0, tiled=True)  30.9 us
    all_gather x1, blocking collectives, local(): lax.all_gather(keys_a, 'sp', axis=0, tiled=True)  30.7 us
    reduce_scatter x1, waiting for transfers between devices, local(): lax.psum_scatter(jnp.dot(hidden, down_whole, preferred_element_type=jnp.f...  23.1 us
    all_gather x1, waiting for transfers between devices, local(): lax.all_gather(normed, 'tp', axis=0, tiled=True)  15.7 us
  transfers between devices with their start and end apart: 8, of which 5 were waited for; matrix products, arithmetic and copies ran while one was open for 4% of the time, Pallas kernels for 0%

commit v1 on v0

--- a/solution.py
+++ b/solution.py
@@ -140,7 +140,7 @@
     ).astype(jnp.bfloat16)
     up_whole, down_whole = (
         lax.all_gather(w_up, "sp", axis=0, tiled=True),
-        lax.all_gather(w_down, "sp", axis=1, tiled=True),
+        jnp.concatenate(lax.all_gather(w_down, "sp"), axis=1),
     )
     hidden = jnp.square(
         jax.nn.relu(

time: 481 us -> 400 us (0.83)
  waiting for transfers between devices: 297 us -> 200 us
  local copies, waits for them, and re-layouts: 3.64 us -> 15.8 us
    all_gather x1, waiting for transfers between devices: 125 us -> 38 us  [local(): lax.all_gather(w_down, 'sp')]
    reshape x0 -> x1, local copies, waits for them, and re-layouts: none -> 11.5 us  [local(): jnp.concatenate(lax.all_gather(w_down, 'sp'), axis=1)]
    all_gather x1, waiting for transfers between devices: 15.7 us -> 5.36 us  [local(): lax.all_gather(normed, 'tp', axis=0, tiled=True)]
  transfers between devices with their start and end apart: 8 -> 8, of which waited for: 5 -> 5; matrix products, arithmetic and copies ran while one was open for 4% -> 9% of each run, Pallas kernels for 0% -> 0%
where the time goes in v1:
time: 400 us
  waiting for transfers between devices  200 us (50%)
  blocking collectives  130 us (32%)
  matrix products  22.2 us (6%)
  local copies, waits for them, and re-layouts  15.8 us (4%)
  between operations  13.9 us (3%)
  other arithmetic  10.6 us (3%)
  starting transfers between devices  6.85 us (2%)
    all_gather x1, waiting for transfers between devices, local(): lax.all_gather(w_up, 'sp', axis=0, tiled=True)  126 us
    all_gather x1, waiting for transfers between devices, local(): lax.all_gather(w_down, 'sp')  38 us
    all_gather x1, blocking collectives, local(): lax.all_gather(keys_b, 'sp', axis=0, tiled=True)  33.2 us
    all_gather x1, blocking collectives, local(): lax.all_gather(keys_a, 'sp', axis=0, tiled=True)  32.8 us
    all_gather x1, blocking collectives, local(): lax.all_gather(values_a, 'sp', axis=0, tiled=True)  32.6 us
    all_gather x1, blocking collectives, local(): lax.all_gather(values_b, 'sp', axis=0, tiled=True)  31.4 us
    reduce_scatter x1, waiting for transfers between devices, local(): lax.psum_scatter(jnp.dot(hidden, down_whole, preferred_element_type=jnp.f...  23.1 us
    dot_general x1, matrix products, local(): jnp.dot(hidden, down_whole, preferred_element_type=jnp.float32)  11.6 us
  transfers between devices with their start and end apart: 8, of which 5 were waited for; matrix products, arithmetic and copies ran while one was open for 9% of the time, Pallas kernels for 0%

profile of v1, /device:TPU:0, one launch (start us, length us, event | category | flops | bytes accessed | tf_op | source)
XLA Modules:
  0.0 399.5 jit_solution(12943859404623174676)
XLA Ops:
  6.5 0.7 all-gather.11.cloned.1.call-update
  7.3 0.7 all-gather.13.cloned.1.call-update
  8.1 0.7 all-gather.19.cloned.1.call-update
  8.8 1.0 reshape.511
  9.8 1.0 fusion.53
  10.8 0.3 multiply_reduce_fusion.1
  11.1 0.7 broadcast_bitcast_fusion
  11.8 0.9 fusion.55
  12.8 0.1 broadcast_multiply_fusion.1
  12.9 0.2 fusion.63
  13.1 0.6 fusion.58
  13.7 33.2 %all-gather.2 = bf16[2048,128]{1,0:T(8,128)(2,1)S(1)} all-gather(bf16[256,128]{1,0:T(8,128)(2,1)S(1)} %get-tuple-element.5), channel_id=4, replica_groups=mesh['sp'=8,'tp'=4] {'sp'}, dimensions={0}, use_global_device_ids=true | all-gather | bytes 589824 | tf_op jit(solution)/shard_map/all_gather | solution.py:119
  47.0 0.3 multiply_multiply_fusion
  47.3 0.9 slice_negate_fusion.1
  48.2 0.9 maximum_multiply_fusion.1
  49.1 0.1 mul.427
  49.2 0.3 mul.420
  49.5 0.7 bitcast_reduce_fusion.1
  50.3 0.7 fusion.7
  51.1 31.4 %all-gather.3 = bf16[2048,128]{1,0:T(8,128)(2,1)S(1)} all-gather(bf16[256,128]{1,0:T(8,128)(2,1)S(1)} %copy-done.5), channel_id=5, replica_groups=mesh['sp'=8,'tp'=4] {'sp'}, dimensions={0}, use_global_device_ids=true | all-gather | bytes 589824 | tf_op jit(solution)/shard_map/all_gather | solution.py:120
  82.5 0.9 fusion.31
  83.4 0.1 copy.58
  83.5 0.7 convert_element_type.140
  84.3 3.3 all-to-all-start.1
  87.6 0.1 copy.50
  88.1 0.1 fusion.69
  88.3 0.1 multiply_multiply_fusion.1
  88.4 0.1 fusion.49
  88.5 32.8 %all-gather = bf16[2048,64]{0,1:T(8,128)(2,1)S(1)} all-gather(bf16[256,64]{0,1:T(8,128)(2,1)S(1)} %get-tuple-element.26), channel_id=2, replica_groups=mesh['sp'=8,'tp'=4] {'sp'}, dimensions={0}, use_global_device_ids=true | all-gather | bytes 294912 | tf_op jit(solution)/shard_map/all_gather | solution.py:112
  121.4 32.6 %all-gather.1 = bf16[2048,64]{0,1:T(8,128)(2,1)S(1)} all-gather(bf16[256,64]{0,1:T(8,128)(2,1)S(1)} %copy-done.6), channel_id=3, replica_groups=mesh['sp'=8,'tp'=4] {'sp'}, dimensions={0}, use_global_device_ids=true | all-gather | bytes 294912 | tf_op jit(solution)/shard_map/all_gather | solution.py:113
  153.9 1.3 bitcast_reduce_fusion
  155.2 1.4 fusion.1
  156.6 1.5 fusion.40
  158.1 0.2 reshape.530
  158.3 0.8 copy.63
  159.1 3.3 all-to-all-start
  162.5 4.5 %all-to-all-done = bf16[4,64,256]{2,1,0:T(8,128)(2,1)S(1)} async-done(((bf16[4,64,256]{2,1,0:T(8,128)(2,1)}), bf16[4,64,256]{2,1,0:T(8,128)(2,1)S(1)}, u32[]{:S(2)}, u32[]{:S(2)}) %all-to-all-start) | async-done | bytes 131104 | tf_op jit(solution)/shard_map/all_to_all | solution.py:126
  167.1 3.0 fusion.86
  170.2 3.2 multiply_reduce_fusion
  173.4 0.8 multiply_convert_fusion
  174.3 0.5 all-gather.17.cloned.1.call-update
  174.8 38.0 %all-gather.19.cloned.1.call-done = bf16[16384,256]{1,0:T(8,128)(2,1)} async-done(((bf16[2048,256]{1,0:T(8,128)(2,1)}), bf16[16384,256]{1,0:T(8,128)(2,1)}) %all-gather.19.cloned.1.call-update) | async-done | bytes 8388624 | tf_op jit(solution)/shard_map/all_gather | solution.py:143
  212.9 11.5 %copy.60 = bf16[2048,8,256]{0,2,1:T(8,128)(2,1)} copy(bf16[2048,8,256]{2,0,1:T(8,128)(2,1)} %bitcast.192) | data formatting | bytes 16777216 | tf_op jit(solution)/shard_map/reshape | solution.py:143
  224.4 5.4 %all-gather.15.cloned.1.call-done = bf16[256,2048]{1,0:T(8,128)(2,1)} async-done(((bf16[64,2048]{1,0:T(8,128)(2,1)}), bf16[256,2048]{1,0:T(8,128)(2,1)}) %all-gather.15.cloned.1.call-update) | async-done | bytes 1048592 | tf_op jit(solution)/shard_map/all_gather | solution.py:148
  229.8 126.5 %all-gather.17.cloned.1.call-done = bf16[2048,2048]{1,0:T(8,128)(2,1)} async-done(((bf16[256,2048]{1,0:T(8,128)(2,1)}), bf16[2048,2048]{1,0:T(8,128)(2,1)}) %all-gather.17.cloned.1.call-update) | async-done | bytes 8388624 | tf_op jit(solution)/shard_map/all_gather | solution.py:142
  356.3 11.6 %convolution_convert_fusion = bf16[256,2048]{1,0:T(8,128)(2,1)} fusion(bf16[2048,2048]{0,1:T(8,128)(2,1)} %bitcast.193, bf16[256,2048]{1,0:T(8,128)(2,1)} %all-gather.15.cloned.1.call-done, bf16[2048,2048]{1,0:T(8,128)(2,1)} %all-gather.17.cloned.1.call-done), kind=kOutput, calls=%fused_computation.15 | convolution fusion | flops 4297064448 | bytes 18874368 | tf_op jit(solution)/shard_map/dot_general | solution.py:155
  367.8 23.1 %reduce-scatter.2.cloned.1.call-done = bf16[64,2048]{1,0:T(8,128)(2,1)} async-done(((bf16[256,2048]{1,0:T(8,128)(2,1)}), bf16[64,2048]{1,0:T(8,128)(2,1)}) %reduce-scatter.2.cloned.1.call-update) | async-done | bytes 262160 | tf_op jit(solution)/shard_map/reduce_scatter | solution.py:154
  391.0 1.7 add_convert_fusion
  (58 shorter events, 0.8 us)
Async XLA Ops:
  6.5 6.5 %copy-start = (bf16[256,128]{1,0:T(8,128)(2,1)S(1)}, bf16[256,128]{1,0:T(8,128)(2,1)}, u32[]{:S(2)}) copy-start(bf16[256,128]{1,0:T(8,128)(2,1)} %param.21) | copy-start | bytes 196612
  6.5 40.4 %copy-start.11 = (f32[128]{0:T(128)S(1)}, f32[128]{0:T(128)}, u32[]{:S(2)}) copy-start(f32[128]{0:T(128)} %param.25) | copy-start | bytes 1540
  6.5 6.5 %copy-start.8 = (f32[128]{0:T(128)S(1)}, f32[128]{0:T(128)}, u32[]{:S(2)}) copy-start(f32[128]{0:T(128)} %param.26) | copy-start | bytes 1540
  6.5 160.5 %all-gather.11.cloned.1.call-start = ((), (), s32[]{:S(2)}) async-start(), calls=%async_computation.3 | async-start | bytes 5242880 | tf_op jit(solution)/shard_map/all_gather | solution.py:130
  7.3 162.9 %all-gather.13.cloned.1.call-start = ((), (), s32[]{:S(2)}) async-start(), calls=%async_computation.4 | async-start | bytes 5242880 | tf_op jit(solution)/shard_map/all_gather | solution.py:131
  8.0 204.9 %all-gather.19.cloned.1.call-start = ((), (), s32[]{:S(2)}) async-start(), calls=%async_computation.8 | async-start | bytes 9437184 | tf_op jit(solution)/shard_map/all_gather | solution.py:143
  12.7 36.8 %copy-start.1 = (bf16[256,256]{1,0:T(8,128)(2,1)S(1)}, bf16[256,256]{1,0:T(8,128)(2,1)}, u32[]{:S(2)}) copy-start(bf16[256,256]{1,0:T(8,128)(2,1)} %param.20) | copy-start | bytes 393220
  49.5 1.5 copy-start.5
  51.0 36.6 %copy-start.4 = (bf16[256,256]{1,0:T(8,128)(2,1)S(1)}, bf16[256,256]{1,0:T(8,128)(2,1)}, u32[]{:S(2)}) copy-start(bf16[256,256]{1,0:T(8,128)(2,1)} %param.17) | copy-start | bytes 393220
  51.0 36.7 %copy-start.10 = (f32[64]{0:T(128)S(1)}, f32[64]{0:T(128)}, u32[]{:S(2)}) copy-start(f32[64]{0:T(128)} %param.23) | copy-start | bytes 772
  51.0 36.8 %copy-start.2 = (bf16[256,64]{0,1:T(8,128)(2,1)S(1)}, bf16[256,64]{0,1:T(8,128)(2,1)}, u32[]{:S(2)}) copy-start(bf16[256,64]{0,1:T(8,128)(2,1)} %param.18) | copy-start | bytes 98308
  51.0 37.0 %copy-start.9 = (f32[64]{0:T(128)S(1)}, f32[64]{0:T(128)}, u32[]{:S(2)}) copy-start(f32[64]{0:T(128)} %param.24) | copy-start | bytes 772
  82.4 38.9 %copy-start.6 = (bf16[256,64]{0,1:T(8,128)(2,1)S(1)}, bf16[256,64]{0,1:T(8,128)(2,1)}, u32[]{:S(2)}) copy-start(bf16[256,64]{0,1:T(8,128)(2,1)} %param.19) | copy-start | bytes 98308
  84.3 74.9 %all-to-all-start.1 = ((bf16[4,64,256]{2,1,0:T(8,128)(2,1)}), bf16[4,64,256]{2,1,0:T(8,128)(2,1)S(1)}, u32[]{:S(2)}, u32[]{:S(2)}) async-start(bf16[4,64,256]{2,1,0:T(8,128)(2,1)} %convert_element_type.140), calls=%async_computation.1 | async-start | bytes 262144 | tf_op jit(solution)/shard_map/all_to_all | solution.py:127
  158.1 12.0 %copy-start.3 = (bf16[64,2048]{1,0:T(8,128)(2,1)S(1)}, bf16[64,2048]{1,0:T(8,128)(2,1)}, u32[]{:S(2)}) copy-start(bf16[64,2048]{1,0:T(8,128)(2,1)} %param.16) | copy-start | bytes 786436
  159.1 7.9 %all-to-all-start = ((bf16[4,64,256]{2,1,0:T(8,128)(2,1)}), bf16[4,64,256]{2,1,0:T(8,128)(2,1)S(1)}, u32[]{:S(2)}, u32[]{:S(2)}) async-start(bf16[4,64,256]{2,1,0:T(8,128)(2,1)} %copy.63), calls=%async_computation | async-start | bytes 262144 | tf_op jit(solution)/shard_map/all_to_all | solution.py:126
  162.5 67.3 %all-gather.15.cloned.1.call-start = ((), (), s32[]{:S(2)}) async-start(), calls=%async_computation.5 | async-start | bytes 1310720 | tf_op jit(solution)/shard_map/all_gather | solution.py:148
  167.1 6.3 %copy-start.7 = (f32[2048]{0:T(1024)S(1)}, f32[2048]{0:T(1024)}, u32[]{:S(2)}) copy-start(f32[2048]{0:T(1024)} %param.29) | copy-start | bytes 24580
  174.2 182.1 %all-gather.17.cloned.1.call-start = ((), (), s32[]{:S(2)}) async-start(), calls=%async_computation.6 | async-start | bytes 9437184 | tf_op jit(solution)/shard_map/all_gather | solution.py:142
  174.8 216.2 %reduce-scatter.2.cloned.1.call-start = ((), (), s32[]{:S(2)}) async-start(), calls=%async_computation.7 | async-start | bytes 1310720 | tf_op jit(solution)/shard_map/reduce_scatter | solution.py:154
Sparse Core Ops, SparseCore 0:
  8.9 37.1 all-gather.10
  47.7 34.4 all-gather.12
  84.3 128.5 all-gather.18
  214.3 15.4 all-gather.14
  231.8 124.4 all-gather.16
  368.0 22.9 reduce-scatter.1
